TPU v7x, 256 devices: a whole 4x4x8 slice. The times are simulated.
256 devices in a mesh: sp: 32 (over z, y), dp: 8 (over x, core).
Axes of the slice: x: 4, y: 4, z: 8, core: 2. Of those that a mesh axis runs over, the one named last changes fastest.
Arguments:
- hidden_states: bfloat16 [16, 4096, 2048], P('dp', 'sp'), may hold values from -288 to 288
- cumulative_gate: float32 [16, 4096, 32], P('dp', 'sp'), may hold values from -16384 to 0, as said below
- query_weight: bfloat16 [2048, 2048], P('dp'), may hold values from -0.125 to 0.125
- key_weight: bfloat16 [2048, 512], P('dp'), may hold values from -0.125 to 0.125
- value_weight: bfloat16 [2048, 512], P('dp'), may hold values from -0.125 to 0.125
- out_weight: bfloat16 [2048, 2048], P('dp'), may hold values from -0.75 to 0.75
Outputs:
- mixed: bfloat16 [16, 4096, 2048], P('dp', 'sp')
Inputs may be any that keep to these rules, and one draw needn't show every extreme that they name: cumulative_gate never rises along a sequence and is at most 0.
All inputs are finite; a program needn't handle non-finite values.
Results may differ from a plain program's by a relative error of at most 0.009.
The roundings to bfloat16 on the way count: a program that leaves them out, or rounds other values in their place, can miss the bound.
Values may be sent and summed in bfloat16 or wider, within the bound.
No kernel may reach another device: no remote copies, remote signals or barrier semaphores. Data moves between devices by JAX's collectives and lax.ppermute only.
A program may use at most 64 MiB of HBM per device.

v0:
```python
import math

import jax
import jax.numpy as jnp
from jax import lax
from jax.sharding import PartitionSpec as P

KV_HEADS = 8
HEAD = 64


def in_one_piece(arrays, axis, dim, along):
    both = jnp.concatenate(arrays, axis=along)
    out, at, gathered = (lax.all_gather(both, axis, axis=dim, tiled=True), 0, [])
    for a in arrays:
        gathered.append(lax.slice_in_dim(out, at, at + a.shape[along], axis=along))
        at += a.shape[along]
    return tuple(gathered)


def attend_one(query_head, key_head, value_head, gate_head):
    length = query_head.shape[0]
    block_rows = math.gcd(length, 512)
    block_count = length // block_rows
    key_index = jnp.arange(length, dtype=jnp.int32)
    scaling = query_head.shape[1] ** (-0.5)

    def one_block(block_number):
        offset = block_number * block_rows
        query_block = lax.dynamic_slice_in_dim(query_head, offset, block_rows, 0)
        gate_block = lax.dynamic_slice_in_dim(gate_head, offset, block_rows, 0)
        scores = jnp.dot(query_block, key_head.T, preferred_element_type=jnp.float32) * scaling
        scores = scores + gate_block[:, None] - gate_head[None, :]
        row_index = offset + jnp.arange(block_rows, dtype=jnp.int32)
        allowed = key_index[None, :] <= row_index[:, None]
        scores = jnp.where(allowed, scores, -jnp.inf)
        maximum = jnp.max(scores, axis=1, keepdims=True)
        exponent = jnp.where(allowed, jnp.exp(scores - maximum), 0.0)
        weights = (exponent / jnp.sum(exponent, axis=1, keepdims=True)).astype(jnp.bfloat16)
        return jnp.dot(weights, value_head, preferred_element_type=jnp.float32).astype(jnp.bfloat16)

    result = lax.map(one_block, jnp.arange(block_count, dtype=jnp.int32))
    return result.reshape(length, query_head.shape[1])


def on_device(hidden_states, cumulative_gate, query_weight, key_weight, value_weight, out_weight):
    sequences, positions, model_width = hidden_states.shape
    token_rows = hidden_states.reshape(sequences * positions, model_width)
    width_query = query_weight.shape[1]
    copies = max(1, lax.axis_size("sp") // KV_HEADS)

    def absorb(portion):
        return jnp.dot(token_rows, portion, preferred_element_type=jnp.float32)

    def spread(matrix):
        matrix = matrix.astype(jnp.bfloat16).reshape(sequences, positions, KV_HEADS, HEAD)
        return jnp.repeat(matrix, copies, axis=2).reshape(
            sequences, positions, KV_HEADS * copies * HEAD
        )

    summed = absorb(lax.all_gather(query_weight, "dp", axis=0, tiled=True))
    query_local = summed.astype(jnp.bfloat16).reshape(sequences, positions, width_query)
    portions = in_one_piece((key_weight, value_weight), "dp", 0, 1)
    key_sum = absorb(portions[0])
    value_sum = absorb(portions[1])
    key_local = spread(key_sum)
    value_local = spread(value_sum)
    query, key, value = (
        lax.all_to_all(query_local, "sp", split_axis=2, concat_axis=1, tiled=True),
        lax.all_to_all(key_local, "sp", split_axis=2, concat_axis=1, tiled=True),
        lax.all_to_all(value_local, "sp", split_axis=2, concat_axis=1, tiled=True),
    )
    gates = lax.all_to_all(cumulative_gate, "sp", split_axis=2, concat_axis=1, tiled=True)
    length = query.shape[1]
    heads_here = query.shape[2] // HEAD
    pairs_here = key.shape[2] // HEAD
    per_group = heads_here // pairs_here
    head_query = query.reshape(sequences, length, pairs_here, per_group, HEAD)
    head_query = jnp.transpose(head_query, (0, 2, 3, 1, 4)).reshape(
        sequences * pairs_here, per_group, length, HEAD
    )
    head_key = jnp.transpose(
        key.reshape(sequences, length, pairs_here, HEAD), (0, 2, 1, 3)
    ).reshape(sequences * pairs_here, length, HEAD)
    head_value = jnp.transpose(
        value.reshape(sequences, length, pairs_here, HEAD), (0, 2, 1, 3)
    ).reshape(sequences * pairs_here, length, HEAD)
    head_gate = jnp.transpose(
        gates.reshape(sequences, length, pairs_here, per_group), (0, 2, 3, 1)
    ).reshape(sequences * pairs_here, per_group, length)

    def per_pair(inputs):
        group_query, group_key, group_value, group_gate = inputs

        def per_head(head_inputs):
            return attend_one(head_inputs[0], group_key, group_value, head_inputs[1])

        return lax.map(per_head, (group_query, group_gate))

    attended = lax.map(per_pair, (head_query, head_key, head_value, head_gate))
    attended = attended.reshape(sequences, pairs_here, per_group, length, HEAD)
    attended = jnp.transpose(attended, (0, 3, 1, 2, 4)).reshape(
        sequences, length, heads_here * HEAD
    )
    returned = lax.all_to_all(attended, "sp", split_axis=1, concat_axis=2, tiled=True)
    returned_rows = returned.reshape(sequences * positions, width_query)
    mixed = jnp.dot(
        returned_rows,
        lax.all_gather(out_weight, "dp", axis=0, tiled=True),
        preferred_element_type=jnp.float32,
    )
    return mixed.astype(jnp.bfloat16).reshape(sequences, positions, model_width)


def solution(mesh):
    placed = (
        P("dp", "sp", None),
        P("dp", "sp", None),
        P("dp", None),
        P("dp", None),
        P("dp", None),
        P("dp", None),
    )
    return jax.shard_map(
        on_device, mesh=mesh, in_specs=placed, out_specs=P("dp", "sp", None), check_vma=False
    )
```

profile of v0, /device:TPU:8, one launch (start us, length us, event | category | flops | bytes accessed | tf_op | source)
XLA Modules:
  0.0 388.7 jit_solution(7051025074717002793)
XLA Ops:
  10.7 11.7 %all-to-all-start.1 = ((f32[2,128,32]{1,0,2:T(2,128)}), f32[2,128,32]{1,0,2:T(2,128)S(1)}, u32[]{:S(2)}, u32[]{:S(2)}) async-start(f32[2,128,32]{1,0,2:T(2,128)} %copy.49), calls=%async_computation.1 | async-start | bytes 65536 | tf_op jit(solution)/shard_map/all_to_all | solution.py:73
  22.4 24.3 %all-gather.6.cloned.1.call-done = bf16[2048,1024]{1,0:T(8,128)(2,1)} async-done(((bf16[256,1024]{1,0:T(8,128)(2,1)}), bf16[2048,1024]{1,0:T(8,128)(2,1)}) %all-gather.6.cloned.1.call-update) | async-done | bytes 4194320 | tf_op jit(solution)/shard_map/all_gather | solution.py:14
  49.4 9.5 %copy.52 = bf16[2,128,2048]{1,0,2:T(2,128)(2,1)} copy(bf16[2,128,2048]{1,2,0:T(8,128)(2,1)S(1)} %bitcast.97) | data formatting | bytes 2097152 | tf_op jit(solution)/shard_map/reshape;reshape | solution.py:57
  58.9 10.2 %all-to-all-start.2 = ((bf16[2,128,2048]{1,0,2:T(2,128)(2,1)}), bf16[2,128,2048]{1,0,2:T(2,128)(2,1)S(1)}, u32[]{:S(2)}, u32[]{:S(2)}) async-start(bf16[2,128,2048]{1,0,2:T(2,128)(2,1)} %copy.52), calls=%async_computation.2 | async-start | bytes 2097152 | tf_op jit(solution)/shard_map/all_to_all | solution.py:70
  71.8 9.5 %copy.56 = bf16[2,128,2048]{1,0,2:T(2,128)(2,1)} copy(bf16[2,128,2048]{1,2,0:T(8,128)(2,1)S(1)} %bitcast.98) | data formatting | bytes 2097152 | tf_op jit(solution)/shard_map/reshape;reshape | solution.py:57
  81.3 16.2 %all-to-all-done.2 = bf16[2,128,2048]{1,0,2:T(2,128)(2,1)S(1)} async-done(((bf16[2,128,2048]{1,0,2:T(2,128)(2,1)}), bf16[2,128,2048]{1,0,2:T(2,128)(2,1)S(1)}, u32[]{:S(2)}, u32[]{:S(2)}) %all-to-all-start.2) | async-done | bytes 1048608 | tf_op jit(solution)/shard_map/all_to_all | solution.py:70
  97.5 5.6 %all-to-all-start.3 = ((bf16[2,128,2048]{1,0,2:T(2,128)(2,1)}), bf16[2,128,2048]{1,0,2:T(2,128)(2,1)S(1)}, u32[]{:S(2)}, u32[]{:S(2)}) async-start(bf16[2,128,2048]{1,0,2:T(2,128)(2,1)} %copy.56), calls=%async_computation.3 | async-start | bytes 2097152 | tf_op jit(solution)/shard_map/all_to_all | solution.py:71
  103.1 6.7 %convolution_convert_fusion.1 = bf16[256,2048]{1,0:T(8,128)(2,1)} fusion(bf16[256,2048]{1,0:T(8,128)(2,1)S(1)} %bitcast.84, bf16[2048,2048]{1,0:T(8,128)(2,1)} %all-gather.4.cloned.1.call-done), kind=kOutput, calls=%fused_computation.20 | convolution fusion | flops 2148007936 | bytes 10485760 | tf_op jit(solution)/shard_map/dot_general | solution.py:53
  109.8 3.7 copy.46
  113.5 16.7 %all-to-all-done.3 = bf16[2,128,2048]{1,0,2:T(2,128)(2,1)S(1)} async-done(((bf16[2,128,2048]{1,0,2:T(2,128)(2,1)}), bf16[2,128,2048]{1,0,2:T(2,128)(2,1)S(1)}, u32[]{:S(2)}, u32[]{:S(2)}) %all-to-all-start.3) | async-done | bytes 1048608 | tf_op jit(solution)/shard_map/all_to_all | solution.py:71
  130.2 5.6 %all-to-all-start = ((bf16[2,128,2048]{1,0,2:T(2,128)(2,1)}), bf16[2,128,2048]{1,0,2:T(2,128)(2,1)}, u32[]{:S(2)}, u32[]{:S(2)}) async-start(bf16[2,128,2048]{1,0,2:T(2,128)(2,1)} %copy.46), calls=%async_computation | async-start | bytes 2097152 | tf_op jit(solution)/shard_map/all_to_all | solution.py:69
  140.5 22.1 %all-to-all-done = bf16[2,128,2048]{1,0,2:T(2,128)(2,1)} async-done(((bf16[2,128,2048]{1,0,2:T(2,128)(2,1)}), bf16[2,128,2048]{1,0,2:T(2,128)(2,1)}, u32[]{:S(2)}, u32[]{:S(2)}) %all-to-all-start) | async-done | bytes 1048608 | tf_op jit(solution)/shard_map/all_to_all | solution.py:69
  165.7 162.7 %while.29 = (s32[]{:T(128)}, bf16[2,1,4096,64]{3,2,1,0:T(8,128)(2,1)}, bf16[2,1,4096,64]{3,2,1,0:T(8,128)(2,1)}, f32[2,1,4096]{2,1,0:T(1,128)S(1)}, bf16[2,4096,...) while((s32[]{:T(128)}, ...), condition=%wide.region_5.6_spmd, body=%wide.region_0.5_spmd.sunk | while | flops 568360448 | bytes 32777652 | solution.py:100
  168.7 75.7 %while.30 = (s32[]{:T(128)}, bf16[8,512,64]{1,2,0:T(8,128)(2,1)}, s32[8]{0:T(128)S(1)}, bf16[4096,64]{1,0:T(8,128)(2,1)S(1)}, bf16[4096,64]{1,0:T(8,128)(2,1)S(1...) while((s32[]{:T(128)}, bf16[8,512,64]{1,2,0:T(8,128)(2,1)}, ...), condition=%wide.region_4.4_spmd.clone, body=%wide.region_1.3_spmd.clone.sunk | while | flops 568360448 | bytes 26976948 | solution.py:42
  174.6 3.6 fusion.48
  184.1 3.6 fusion.48
  212.5 3.6 fusion.48
  240.9 3.6 fusion.48
  250.1 75.7 %while.30 = (s32[]{:T(128)}, bf16[8,512,64]{1,2,0:T(8,128)(2,1)}, s32[8]{0:T(128)S(1)}, bf16[4096,64]{1,0:T(8,128)(2,1)S(1)}, bf16[4096,64]{1,0:T(8,128)(2,1)S(1...) while((s32[]{:T(128)}, bf16[8,512,64]{1,2,0:T(8,128)(2,1)}, ...), condition=%wide.region_4.4_spmd.clone, body=%wide.region_1.3_spmd.clone.sunk | while | flops 568360448 | bytes 26976948 | solution.py:42
  274.9 3.6 fusion.48
  328.4 4.8 %copy.78 = bf16[2,1,4096,64]{3,0,2,1:T(2,128)(2,1)S(1)} copy(bf16[2,1,4096,64]{3,2,1,0:T(8,128)(2,1)} %get-tuple-element.97) | data formatting | bytes 2097152 | tf_op jit(solution)/shard_map/while | solution.py:100
  334.6 32.0 %all_to_all.81 = bf16[32,2,8192]{2,1,0:T(2,128)(2,1)} all-to-all(bf16[32,2,8192]{2,1,0:T(2,128)(2,1)S(1)} %reshape.44), channel_id=1, replica_groups=mesh['sp'=32,'dp'=8] {'sp'}, dimensions={0} | all-to-all | bytes 2097152 | tf_op jit(solution)/shard_map/all_to_all | solution.py:105
  366.7 5.0 %reshape.45 = bf16[4096,2,64]{2,1,0:T(2,128)(2,1)S(1)} reshape(bf16[32,2,8192]{2,1,0:T(2,128)(2,1)} %all_to_all.81) | data formatting | bytes 2097152
  375.1 7.0 %convolution_convert_fusion = bf16[256,2048]{1,0:T(8,128)(2,1)} fusion(bf16[2048,2048]{1,0:T(8,128)(2,1)} %all-gather.8.cloned.1.call-done, bf16[256,8,2,128]{3,2,1,0:T(2,128)(2,1)} %bitcast.93), kind=kOutput, calls=%fused_computation.19 | convolution fusion | flops 2148007936 | bytes 10485760 | tf_op jit(solution)/shard_map/dot_general | solution.py:107
  (138 shorter events, 157.9 us)
Async XLA Ops:
  6.5 40.1 %copy-start = (bf16[2,128,2048]{2,1,0:T(8,128)(2,1)S(1)}, bf16[2,128,2048]{2,1,0:T(8,128)(2,1)}, u32[]{:S(2)}) copy-start(bf16[2,128,2048]{2,1,0:T(8,128)(2,1)} %param.10) | copy-start | bytes 3145732
  6.5 40.1 %all-gather.6.cloned.1.call-start = ((), (), s32[]{:S(2)}) async-start(), calls=%async_computation.6 | async-start | bytes 4718592 | tf_op jit(solution)/shard_map/all_gather | solution.py:14
  8.5 94.6 %all-gather.4.cloned.1.call-start = ((), (), s32[]{:S(2)}) async-start(), calls=%async_computation.5 | async-start | bytes 9437184 | tf_op jit(solution)/shard_map/all_gather | solution.py:61
  10.7 48.2 %all-to-all-start.1 = ((f32[2,128,32]{1,0,2:T(2,128)}), f32[2,128,32]{1,0,2:T(2,128)S(1)}, u32[]{:S(2)}, u32[]{:S(2)}) async-start(f32[2,128,32]{1,0,2:T(2,128)} %copy.49), calls=%async_computation.1 | async-start | bytes 65536 | tf_op jit(solution)/shard_map/all_to_all | solution.py:73
  58.9 38.6 %all-to-all-start.2 = ((bf16[2,128,2048]{1,0,2:T(2,128)(2,1)}), bf16[2,128,2048]{1,0,2:T(2,128)(2,1)S(1)}, u32[]{:S(2)}, u32[]{:S(2)}) async-start(bf16[2,128,2048]{1,0,2:T(2,128)(2,1)} %copy.52), calls=%async_computation.2 | async-start | bytes 2097152 | tf_op jit(solution)/shard_map/all_to_all | solution.py:70
  97.5 32.7 %all-to-all-start.3 = ((bf16[2,128,2048]{1,0,2:T(2,128)(2,1)}), bf16[2,128,2048]{1,0,2:T(2,128)(2,1)S(1)}, u32[]{:S(2)}, u32[]{:S(2)}) async-start(bf16[2,128,2048]{1,0,2:T(2,128)(2,1)} %copy.56), calls=%async_computation.3 | async-start | bytes 2097152 | tf_op jit(solution)/shard_map/all_to_all | solution.py:71
  130.2 32.4 %all-to-all-start = ((bf16[2,128,2048]{1,0,2:T(2,128)(2,1)}), bf16[2,128,2048]{1,0,2:T(2,128)(2,1)}, u32[]{:S(2)}, u32[]{:S(2)}) async-start(bf16[2,128,2048]{1,0,2:T(2,128)(2,1)} %copy.46), calls=%async_computation | async-start | bytes 2097152 | tf_op jit(solution)/shard_map/all_to_all | solution.py:69
  135.8 239.3 %all-gather.8.cloned.1.call-start = ((), (), s32[]{:S(2)}) async-start(), calls=%async_computation.7 | async-start | bytes 9437184 | tf_op jit(solution)/shard_map/all_gather | solution.py:109
  371.7 10.5 %copy-start.1 = (bf16[2,128,2048]{2,1,0:T(8,128)(2,1)S(1)}, bf16[2,128,2048]{2,1,0:T(8,128)(2,1)}, u32[]{:S(2)}) copy-start(bf16[2,128,2048]{2,1,0:T(8,128)(2,1)} %param.10) | copy-start | bytes 3145732
Sparse Core Ops, SparseCore 0:
  9.2 37.4 all-gather.5
  48.5 52.1 all-gather.3
  138.5 51.7 all-gather.7
where the time goes:
time: 390 us; the launch traced here: 389 us
  matrix products  112 us (29%)
  waiting for transfers between devices  80.5 us (21%)
  local copies, waits for them, and re-layouts  67.7 us (17%)
  other arithmetic  40.4 us (10%)
  starting transfers between devices  33.4 us (9%)
  blocking collectives  32 us (8%)
  between operations  13.3 us (3%)
  loops' own time  9.06 us (2%)
    dot_general x16, matrix products, one_block(): jnp.dot(weights, value_head, preferred_element_type=jnp.float32)  57.3 us
    reduce_sum x16, other arithmetic, one_block(): jnp.sum(exponent, axis=1, keepdims=True)  38.4 us
    dot_general x16, matrix products, one_block(): jnp.dot(query_block, key_head.T, preferred_element_type=jnp.float32)  36.6 us
    all_to_all x1, blocking collectives, on_device(): lax.all_to_all(attended, 'sp', split_axis=1, concat_axis=2, tiled=True)  32 us
    all_gather x1, waiting for transfers between devices, in_one_piece(): lax.all_gather(both, axis, axis=dim, tiled=True)  24.3 us
    all_to_all x1, waiting for transfers between devices, on_device(): lax.all_to_all(query_local, 'sp', split_axis=2, concat_axis=1, tiled=True)  22.1 us
    another operation x2, local copies, waits for them, and re-layouts, spread(): jnp.repeat(matrix, copies, axis=2)  18.9 us
    all_to_all x1, waiting for transfers between devices, on_device(): lax.all_to_all(value_local, 'sp', split_axis=2, concat_axis=1, tiled=True)  16.7 us
  transfers between devices with their start and end apart: 7, of which 4 were waited for; matrix products, arithmetic and copies ran while one was open for 54% of the time, Pallas kernels for 0%

commit v1 on v0

v1 whole, which is shorter than its diff:
```python
import functools

import jax
import jax.numpy as jnp
from jax import lax
from jax.experimental import pallas as pl
from jax.experimental.pallas import tpu as pltpu
from jax.sharding import Mesh
from jax.sharding import PartitionSpec as P

Z, X = 8, 4
GROUPS = 8
POS = 128
BLOCKS = 32
UNITS = 16
LENGTH = BLOCKS * POS
TILE = 512
PART = 256
NEG = -1e30
VMEM = pl.BlockSpec(memory_space=pltpu.VMEM)
SMEM = pl.BlockSpec(memory_space=pltpu.SMEM)


def shift(value, by):
    return lax.ppermute(value, "x", [(i, (i + by) % X) for i in range(X)])


def swap(value, axis="core"):
    return lax.ppermute(value, axis, [(0, 1), (1, 0)])


def exchange(value, axes):
    return lax.all_to_all(value, axes, 0, 0, tiled=True)


def gather_x(own):
    half = own.shape[0] // 2
    before = shift(own, 1)
    after = shift(own, -1)
    low = shift(before[:half], 1)
    high = shift(after[half:], -1)
    return own, before, after, low, high


def fetch_x(own):
    return (own, shift(own, 1), shift(own, -1), shift(own, 2))


def call(kernel, flops, mebibytes=16, **arguments):
    return pl.pallas_call(
        kernel,
        compiler_params=pltpu.CompilerParams(vmem_limit_bytes=mebibytes << 20),
        cost_estimate=pl.CostEstimate(flops=flops, bytes_accessed=4 << 20, transcendentals=0),
        **arguments,
    )


def arrange_kernel(where_ref, query_ref, keep, give):
    c = where_ref[1]
    p = where_ref[2]
    first = c == 0
    for g in range(4):
        at = pl.multiple_of(p * 1024 + g * 256, 256)
        low = query_ref[:, pl.ds(at, 128)]
        high = query_ref[:, pl.ds(at + 128, 128)]
        keep[:, g * 128 : g * 128 + 128] = jnp.where(first, low, high)
        give[:, g * 128 : g * 128 + 128] = jnp.where(first, high, low)


def arrange(where, wq):
    shape = jax.ShapeDtypeStruct((256, 512), jnp.bfloat16)
    return call(
        arrange_kernel, 1 << 20, out_shape=(shape,) * 2,
        in_specs=[SMEM, VMEM], out_specs=(VMEM,) * 2,
    )(where, wq)


def pieces_of(where_ref, refs):
    x = where_ref[0]
    c = where_ref[1]
    pieces = []
    for step, ref, flips in zip((0, 3, 1, 2, 2), refs, ((0, 1), (0, 1), (0, 1), (0, 1), (1,))):
        for flip in flips[: ref.shape[0] // 256]:
            column = (lax.rem(x + step, X) * 2 + (1 - c if flip else c)) * 256
            pieces.append((pl.multiple_of(column, 256), ref, 256 * (len(flips) - 1) * flip))
    return pieces


def product(tokens, pieces, columns):
    total = None
    for column, ref, row in pieces:
        part = jnp.dot(
            tokens[:, pl.ds(column, 256)], ref[row : row + 256, columns],
            preferred_element_type=jnp.float32,
        )
        total = part if total is None else total + part
    return total


def project_kv_kernel(where_ref, t0, t1, gate_ref, w0, w1, w2, w3, w4, out_ref):
    c = where_ref[1]
    pieces = pieces_of(where_ref, (w0, w1, w2, w3, w4))
    row = lax.broadcasted_iota(jnp.int32, (16, POS), 0)
    for ref, core in ((t0, c), (t1, 1 - c)):
        for p in range(2):
            total = product(ref, pieces, slice(p * 256, p * 256 + 256))
            for s in range(2):
                flipped = total[s * POS : s * POS + POS].T.astype(jnp.bfloat16)
                for g in range(4):
                    unit = (core * 2 + s) * GROUPS + g * 2 + p
                    out_ref[unit, 0:64] = flipped[g * 64 : g * 64 + 64]
    for u in range(BLOCKS):
        minus = -gate_ref[u]
        high = minus.astype(jnp.bfloat16).astype(jnp.float32)
        rest = minus - high
        middle = rest.astype(jnp.bfloat16).astype(jnp.float32)
        low = rest - middle
        extra = jnp.zeros((16, POS), jnp.float32)
        for h in range(2):
            for k, part in enumerate((high, middle, low)):
                extra = jnp.where(row == 3 * h + k, part[h : h + 1], extra)
        out_ref[u, 64:80] = extra.astype(jnp.bfloat16)


def project_kv(where, tokens, gates, weights):
    return call(
        project_kv_kernel, 2 * 512 * 2048 * 512,
        out_shape=jax.ShapeDtypeStruct((BLOCKS, 80, POS), jnp.bfloat16),
        in_specs=[SMEM] + [VMEM] * 8, out_specs=VMEM,
    )(where, *tokens, gates, *weights)


def project_q_kernel(where_ref, t0, t1, t2, t3, w0, w1, w2, w3, out_ref):
    c = where_ref[1]
    p = where_ref[2]
    pieces = pieces_of(where_ref, (w0, w1, w2, w3))
    for ref, core, side in ((t0, c, p), (t1, 1 - c, p), (t2, c, 1 - p), (t3, 1 - c, 1 - p)):
        at = pl.multiple_of(side * POS, POS)
        for n in range(2):
            total = product(ref, pieces, slice(n * 256, n * 256 + 256)) * 0.125
            for s in range(2):
                flipped = total[s * POS : s * POS + POS].T.astype(jnp.bfloat16)
                unit = (core * 2 + s) * 4 + n * 2
                for k in range(2):
                    out_ref[unit + k, :, pl.ds(at, POS)] = flipped[k * 128 : k * 128 + 128]


def project_q(where, tokens, weights):
    return call(
        project_q_kernel, 2 * 1024 * 2048 * 512,
        out_shape=jax.ShapeDtypeStruct((UNITS, 128, 2 * POS), jnp.bfloat16),
        in_specs=[SMEM] + [VMEM] * 8, out_specs=VMEM,
    )(where, *tokens, *weights)


def attend_kernel(
    where_ref, q_ref, mine_ref, theirs_ref, out_ref,
    keys, values, query, scores, peak, top, total,
):
    blocks = LENGTH // TILE
    per = TILE // POS
    first = where_ref[1] == 0
    row = lax.broadcasted_iota(jnp.int32, (16, POS), 0)
    ones = jnp.where(row == 0, 1.0, 0.0).astype(jnp.bfloat16)
    rest = jnp.zeros((48, POS), jnp.bfloat16)
    for j in range(BLOCKS):
        mine = mine_ref[j, 0:64]
        theirs = theirs_ref[j]
        key = jnp.where(first, mine, theirs)
        whole = jnp.concatenate([key, mine_ref[j, 64:80], rest], axis=0)
        at = slice(j * POS, j * POS + POS)
        keys[at, :] = whole.astype(jnp.float32).T.astype(jnp.bfloat16)
        values[0:64, at] = jnp.where(first, theirs, mine)
        values[64:80, at] = ones
    row = lax.broadcasted_iota(jnp.int32, (64, 2 * POS), 0)
    for h in range(2):
        ones = jnp.where((row >= 3 * h) & (row < 3 * h + 3), 1.0, 0.0).astype(jnp.bfloat16)
        for b in range(UNITS):
            at = slice(b * 2 * POS, b * 2 * POS + 2 * POS)
            query[h, 0:64, at] = q_ref[b, h * 64 : h * 64 + 64]
            query[h, 64:128, at] = ones

    def score(h, i, j, slot, diagonal, r):
        s = jnp.dot(
            keys[pl.ds(pl.multiple_of(j * TILE + r * PART, PART), PART), :],
            query[h, :, pl.ds(pl.multiple_of(i * TILE, TILE), TILE)],
            preferred_element_type=jnp.float32,
        )
        if diagonal:
            a = lax.broadcasted_iota(jnp.int32, (PART, TILE), 0)
            b = lax.broadcasted_iota(jnp.int32, (PART, TILE), 1)
            s = jnp.where(a + r * PART <= b, s, NEG)
        scores[slot, r * PART : r * PART + PART] = s
        m = jnp.max(s, axis=0, keepdims=True)
        peak[slot] = m if r == 0 else jnp.maximum(peak[slot], m)

    def begin(j, slot):
        before = jnp.where(j == 0, NEG, top[...])
        now = jnp.maximum(before, peak[slot])
        top[...] = now
        total[...] = total[...] * jnp.exp(before - now)

    def add(j, slot, r):
        p = jnp.exp(scores[slot, r * PART : r * PART + PART] - top[...]).astype(jnp.bfloat16)
        total[...] += jnp.dot(
            values[:, pl.ds(pl.multiple_of(j * TILE + r * PART, PART), PART)], p,
            preferred_element_type=jnp.float32,
        )

    def finish(h, i):
        result = (total[0:64] / total[64:65]).astype(jnp.bfloat16)
        row = pl.multiple_of(h * 64, 64)
        for b in range(per):
            out_ref[i * per + b, pl.ds(row, 64), :] = result[:, b * POS : b * POS + POS]

    total[...] = jnp.zeros(total.shape, jnp.float32)
    top[...] = jnp.full(top.shape, NEG, jnp.float32)
    for r in range(TILE // PART):
        score(0, 0, 0, 0, True, r)

    def one(h, i, j, slot):
        last = j == i
        over = last & (i == blocks - 1)
        later_h = jnp.where(over, h + 1, h)
        later_i = jnp.where(over, 0, jnp.where(last, i + 1, i))
        later_j = jnp.where(last, 0, j + 1)
        safe_h = jnp.minimum(later_h, 1)

        def go(diagonal):
            begin(j, slot)
            for r in range(TILE // PART):
                score(safe_h, later_i, later_j, 1 - slot, diagonal, r)
                add(j, slot, r)

        @pl.when(later_i == later_j)
        def _():
            go(True)

        @pl.when(later_i != later_j)
        def _():
            go(False)

        @pl.when(last)
        def _():
            finish(h, i)

        return later_h, later_i, later_j

    def two(_, carry):
        return one(*one(*carry, 0), 1)

    zero = jnp.int32(0)
    lax.fori_loop(0, blocks * (blocks + 1) // 2, two, (zero, zero, zero))


def attend(where, query, mine, theirs):
    return call(
        attend_kernel, 4 * LENGTH * LENGTH * 256,
        out_shape=jax.ShapeDtypeStruct((BLOCKS, 128, POS), jnp.bfloat16),
        in_specs=[SMEM] + [VMEM] * 3, out_specs=VMEM,
        scratch_shapes=[
            pltpu.VMEM((LENGTH, 128), jnp.bfloat16),
            pltpu.VMEM((80, LENGTH), jnp.bfloat16),
            pltpu.VMEM((2, 128, LENGTH), jnp.bfloat16),
            pltpu.VMEM((2, TILE, TILE), jnp.float32),
            pltpu.VMEM((2, 1, TILE), jnp.float32),
            pltpu.VMEM((1, TILE), jnp.float32),
            pltpu.VMEM((80, TILE), jnp.float32),
        ],
    )(where, query, mine, theirs)


def mix_kernel(own, where_ref, back, w0, w1, w2, w3, out_ref, left):
    x = where_ref[0]
    c = where_ref[1]
    base = 2 * (c if own else 1 - c)

    @pl.when(pl.program_id(0) == 0)
    def _():
        for k, step in enumerate((0, 3, 1, 2)):
            chip = lax.rem(x + step, X)
            for s in range(2):
                unit = (base + s) * GROUPS + lax.rem(chip, 2) * 4 + lax.div(chip, 2)
                block = jnp.concatenate([back[unit], back[unit + 2]], axis=0)
                block = block.astype(jnp.float32).T.astype(jnp.bfloat16)
                left[k, s * POS : s * POS + POS] = block

    total = None
    for k, ref in enumerate((w0, w1, w2, w3)):
        part = jnp.dot(left[k], ref[...], preferred_element_type=jnp.float32)
        total = part if total is None else total + part
    out_ref[...] = total.astype(out_ref.dtype)


def mix(own, where, back, weights):
    part = pl.BlockSpec((256, 512), lambda n: (0, n))
    return call(
        functools.partial(mix_kernel, own), 2 * 256 * 1024 * 2048,
        grid=(4,),
        out_shape=jax.ShapeDtypeStruct((256, 2048), jnp.float32 if own else jnp.bfloat16),
        in_specs=[SMEM, VMEM] + [part] * 4, out_specs=part,
        scratch_shapes=[pltpu.VMEM((4, 256, 256), jnp.bfloat16)],
    )(where, back, *weights)


def after(value, *others):
    return lax.optimization_barrier((value, *others))[0]


def layer(hidden, gate, wq, wk, wv, wo):
    x = lax.axis_index("x")
    c = lax.axis_index("core")
    first = c == 0
    where = jnp.stack([x, c, lax.axis_index("yl")]).astype(jnp.int32)
    own = hidden.reshape(256, 2048)
    homes = ("z", "yh", "yl")

    beside = swap(own, "yl")
    shard = jnp.concatenate([jnp.where(first, wk, wv), swap(jnp.where(first, wv, wk))], axis=0)
    kv_weights = gather_x(shard)
    keep, give = arrange(where, wq)
    shard = jnp.concatenate([keep, swap(give)], axis=0)
    q_weights = fetch_x(after(shard, kv_weights[1], kv_weights[2]))
    other = swap(own)

    by_unit = jnp.transpose(gate.reshape(2, POS, 2, 4, 2, 2), (4, 0, 3, 2, 5, 1))
    mine = jnp.where(first, by_unit[0], by_unit[1])
    got = swap(jnp.where(first, by_unit[1], by_unit[0]))
    gates = jnp.where(first, jnp.stack([mine, got]), jnp.stack([got, mine]))
    gates = gates.reshape(BLOCKS, 2, POS)

    kv = project_kv(where, (own, other), gates, kv_weights)
    kv = exchange(kv, homes)
    tokens = (own, other, beside, swap(beside))
    query = project_q(where, tokens, q_weights)
    theirs = swap(kv[:, :64])
    query = exchange(query, ("z", "yh"))

    halves = wo.reshape(2, 128, 2048)
    mine = jnp.where(first, halves[0], halves[1])
    got = swap(jnp.where(first, halves[1], halves[0]))
    shard = jnp.where(first, jnp.concatenate([mine, got]), jnp.concatenate([got, mine]))
    o_weights = fetch_x(after(shard, *q_weights[1:]))

    back = exchange(attend(where, query, kv, theirs), homes)
    theirs = swap(mix(False, where, back, o_weights))
    mine = mix(True, where, back, o_weights)
    mixed = mine + theirs.astype(jnp.float32)
    return mixed.astype(jnp.bfloat16).reshape(2, POS, 2048)


def solution(mesh):
    fine = Mesh(mesh.devices.reshape(Z, 2, 2, X, 2), ("z", "yh", "yl", "x", "core"))
    dp, sp = ("x", "core"), ("z", "yh", "yl")
    placed = (P(dp, sp, None), P(dp, sp, None), P(dp, None), P(dp, None), P(dp, None), P(dp, None))
    return jax.shard_map(
        layer, mesh=fine, in_specs=placed, out_specs=P(dp, sp, None), check_vma=False
    )
```

time: 390 us -> 216 us (0.55)
  matrix products: 112 us -> 0 us
  local copies, waits for them, and re-layouts: 67.7 us -> 6.41 us
  Pallas kernels: 0 us -> 44.2 us
  other arithmetic: 40.4 us -> 2.91 us
  waiting for transfers between devices: 80.5 us -> 117 us
  blocking collectives: 32 us -> 0 us
  between operations: 13.3 us -> 0.22 us
  starting transfers between devices: 33.4 us -> 44.1 us
  loops' own time: 9.06 us -> 0 us
    dot_general x36 -> x0, matrix products: 112 us -> none  [the longest x16 57.3 us: one_block(): jnp.dot(weights, value_head, preferred_element_type=jnp.float32)]
    ppermute x0 -> x19, waiting for transfers between devices: none -> 88.8 us  [the longest x10 81.7 us: shift(): return lax.ppermute(value, 'x', [(i, (i + by) % X) for i in range(X)])]
    pallas_call x0 -> x6, Pallas kernels: none -> 44.2 us  [the longest x1 29.1 us: attend(): call(attend_kernel, 4 * LENGTH * LENGTH * 256, out_shape=jax.ShapeDtypeSt...]
    reduce_sum x16 -> x0, other arithmetic: 38.4 us -> none  [one_block(): jnp.sum(exponent, axis=1, keepdims=True)]
    all_to_all x1 -> x0, blocking collectives: 32 us -> none  [on_device(): lax.all_to_all(attended, 'sp', split_axis=1, concat_axis=2, tiled=True)]
    all_to_all x4 -> x3, waiting for transfers between devices: 55 us -> 27.7 us  [exchange(): return lax.all_to_all(value, axes, 0, 0, tiled=True)]
    all_gather x3 -> x0, waiting for transfers between devices: 24.3 us -> none  [the longest x1 24.3 us: in_one_piece(): lax.all_gather(both, axis, axis=dim, tiled=True)]
    ppermute x0 -> x19, starting transfers between devices: none -> 19 us  [the longest x10 15.2 us: shift(): return lax.ppermute(value, 'x', [(i, (i + by) % X) for i in range(X)])]
  transfers between devices with their start and end apart: 7 -> 22, of which waited for: 4 -> 14; matrix products, arithmetic and copies ran while one was open for 54% -> 1% of each run, Pallas kernels for 0% -> 6%
where the time goes in v1:
time: 216 us; the launch traced here: 214 us
  waiting for transfers between devices  117 us (54%)
  Pallas kernels  44.2 us (20%)
  starting transfers between devices  44.1 us (20%)
  local copies, waits for them, and re-layouts  6.41 us (3%)
  other arithmetic  2.91 us (1%)
    ppermute x10, waiting for transfers between devices, shift(): return lax.ppermute(value, 'x', [(i, (i + by) % X) for i in range(X)])  81.7 us
    pallas_call x1, Pallas kernels, attend(): call(attend_kernel, 4 * LENGTH * LENGTH * 256, out_shape=jax.ShapeDtypeSt...  29.1 us
    all_to_all x3, waiting for transfers between devices, exchange(): return lax.all_to_all(value, axes, 0, 0, tiled=True)  27.7 us
    all_to_all x3, starting transfers between devices, exchange(): return lax.all_to_all(value, axes, 0, 0, tiled=True)  25.1 us
    ppermute x10, starting transfers between devices, shift(): return lax.ppermute(value, 'x', [(i, (i + by) % X) for i in range(X)])  15.2 us
    ppermute x9, waiting for transfers between devices, swap(): return lax.ppermute(value, axis, [(0, 1), (1, 0)])  7.08 us
    pallas_call x2, Pallas kernels, mix(): call(functools.partial(mix_kernel, own), 2 * 256 * 1024 * 2048, grid=(4,)...  5.91 us
    unnamed x16, local copies, waits for them, and re-layouts  5.61 us
  transfers between devices with their start and end apart: 22, of which 14 were waited for; matrix products, arithmetic and copies ran while one was open for 1% of the time, Pallas kernels for 6%

profile of v1, /device:TPU:8, one launch (start us, length us, event | category | flops | bytes accessed | tf_op | source)
XLA Modules:
  0.0 214.4 jit_solution(5175293079947715559)
XLA Ops:
  2.8 1.6 collective-permute-start.5
  4.4 1.7 collective-permute-start.6
  6.1 2.2 %collective-permute-start.1 = (bf16[256,2048]{1,0:T(8,128)(2,1)S(1)}, bf16[256,2048]{1,0:T(8,128)(2,1)}, u32[]{:S(2)}, u32[]{:S(2)}) collective-permute-start(bf16[256,2048]{1,0:T(8,128)(2,1)S(1)} %bitcast.14), channel_id=1, source_target_pairs={{0,8},{8,0},{1,9},{9,1},{2,10},{10,2},{3,11},{11,3},{4,12},{12,4},... | collective-permute-start | bytes 3145736 | tf_op jit(solution)/shard_map/ppermute | solution.py:29
  8.3 9.8 %collective-permute-done.5.w1 = bf16[512,512]{1,0:T(8,128)(2,1)S(1)} collective-permute-done((bf16[512,512]{1,0:T(8,128)(2,1)S(1)}, bf16[512,512]{1,0:T(8,128)(2,1)S(1)}, u32[]{:S(2)}, u32[]{:S(2)}) %collective-permute-start.5) | collective-permute-done | bytes 524320 | tf_op jit(solution)/shard_map/ppermute | solution.py:25
  19.2 3.0 %collective-permute-start.12 = (bf16[256,512]{1,0:T(8,128)(2,1)}, bf16[256,512]{1,0:T(8,128)(2,1)S(1)}, u32[]{:S(2)}, u32[]{:S(2)}) collective-permute-start(bf16[256,512]{1,0:T(8,128)(2,1)} %slice.37), channel_id=1, source_target_pairs={{0,6},{2,0},{4,2},{6,4},{1,7},{3,1},{5,3},{7,5},{8,14},{10,8},{12,... | collective-permute-start | bytes 786440 | tf_op jit(solution)/shard_map/ppermute | solution.py:25
  23.5 3.4 %collective-permute-done.11.w3 = bf16[256,512]{1,0:T(8,128)(2,1)S(1)} collective-permute-done((bf16[256,512]{1,0:T(8,128)(2,1)S(1)}, bf16[256,512]{1,0:T(8,128)(2,1)S(1)}, u32[]{:S(2)}, u32[]{:S(2)}) %collective-permute-start.11) | collective-permute-done | bytes 262176 | tf_op jit(solution)/shard_map/ppermute | solution.py:25
  27.2 3.5 %shard_map.66 = bf16[32,80,128]{2,1,0:T(8,128)(2,1)} custom-call(s32[3]{0:T(128)S(1)} %pad_add_fusion.where_ref, bf16[256,2048]{1,0:T(8,128)(2,1)S(1)} %bitcast.15, bf16[256,2048]{1,0:T(8,128)(2,1)} %collective-permute-done.t1, f32[32,2,128]{2,1,0:T(2,128)S(1)} %bitcast.17, bf16[512,512]{1,0:T(8,128)(2,1)S(1)} %pad_maximum_fusion.1.w0, ...), custom_call_target="tpu_custom_call" | custom-call | flops 1073741824 | bytes 4194304 | tf_op jit(solution)/shard_map/pallas_call | solution.py:126
  30.7 11.7 %all-to-all-start.1 = ((bf16[32,80,128]{2,1,0:T(8,128)(2,1)}), bf16[32,80,128]{2,1,0:T(8,128)(2,1)S(1)}, u32[]{:S(2)}, u32[]{:S(2)}) async-start(bf16[32,80,128]{2,1,0:T(8,128)(2,1)} %shard_map.66), calls=%async_computation.1 | async-start | bytes 1310720 | tf_op jit(solution)/shard_map/all_to_all | solution.py:33
  47.3 2.7 %collective-permute-start.8 = (bf16[512,512]{1,0:T(8,128)(2,1)S(1)}, bf16[512,512]{1,0:T(8,128)(2,1)S(1)}, u32[]{:S(2)}, u32[]{:S(2)}) collective-permute-start(bf16[512,512]{1,0:T(8,128)(2,1)S(1)} %pad_maximum_fusion.w0), channel_id=1, source_target_pairs={{0,6},{2,0},{4,2},{6,4},{1,7},{3,1},{5,3},{7,5},{8,14},{10,8},{12,... | collective-permute-start | bytes 1572872 | tf_op jit(solution)/shard_map/ppermute | solution.py:25
  51.3 11.0 %collective-permute-done.7.w1 = bf16[512,512]{1,0:T(8,128)(2,1)S(1)} collective-permute-done((bf16[512,512]{1,0:T(8,128)(2,1)S(1)}, bf16[512,512]{1,0:T(8,128)(2,1)S(1)}, u32[]{:S(2)}, u32[]{:S(2)}) %collective-permute-start.7) | collective-permute-done | bytes 524320 | tf_op jit(solution)/shard_map/ppermute | solution.py:25
  62.3 10.6 %collective-permute-done.8.w2 = bf16[512,512]{1,0:T(8,128)(2,1)S(1)} collective-permute-done((bf16[512,512]{1,0:T(8,128)(2,1)S(1)}, bf16[512,512]{1,0:T(8,128)(2,1)S(1)}, u32[]{:S(2)}, u32[]{:S(2)}) %collective-permute-start.8) | collective-permute-done | bytes 524320 | tf_op jit(solution)/shard_map/ppermute | solution.py:25
  72.9 1.8 collective-permute-done.9.w3
  74.8 5.0 %shard_map.65 = bf16[16,128,256]{2,1,0:T(8,128)(2,1)} custom-call(s32[3]{0:T(128)S(1)} %pad_add_fusion.where_ref, bf16[256,2048]{1,0:T(8,128)(2,1)S(1)} %bitcast.16, bf16[256,2048]{1,0:T(8,128)(2,1)} %collective-permute-done.t1, bf16[256,2048]{1,0:T(8,128)(2,1)} %collective-permute-done.1.t2, bf16[256,2048]{1,0:T(8,128)(2,1)S(1)} %collective-permute-done.2.t3, ...), custom_call_target="tpu_custom_call" | custom-call | flops 2147483648 | bytes 4194304 | tf_op jit(solution)/shard_map/pallas_call | solution.py:149
  79.8 8.3 %all-to-all-start = ((bf16[16,128,256]{2,1,0:T(8,128)(2,1)}), bf16[16,128,256]{2,1,0:T(8,128)(2,1)S(1)}, u32[]{:S(2)}, u32[]{:S(2)}) async-start(bf16[16,128,256]{2,1,0:T(8,128)(2,1)} %shard_map.65), calls=%async_computation | async-start | bytes 2097152 | tf_op jit(solution)/shard_map/all_to_all | solution.py:33
  88.2 1.9 collective-permute-done.13.theirs_ref
  90.1 27.7 %all-to-all-done.q_ref = bf16[16,128,256]{2,1,0:T(8,128)(2,1)S(1)} async-done(((bf16[16,128,256]{2,1,0:T(8,128)(2,1)}), bf16[16,128,256]{2,1,0:T(8,128)(2,1)S(1)}, u32[]{:S(2)}, u32[]{:S(2)}) %all-to-all-start) | async-done | bytes 1048608 | tf_op jit(solution)/shard_map/all_to_all | solution.py:33
  117.8 29.1 %shard_map.67 = bf16[32,128,128]{2,1,0:T(8,128)(2,1)} custom-call(s32[3]{0:T(128)S(1)} %pad_add_fusion.where_ref, bf16[16,128,256]{2,1,0:T(8,128)(2,1)S(1)} %all-to-all-done.q_ref, bf16[32,80,128]{2,1,0:T(8,128)(2,1)S(1)} %all-to-all-done.1.mine_ref, bf16[32,64,128]{2,1,0:T(8,128)(2,1)S(1)} %collective-permute-done.13.theirs_ref), custom_call_target="tpu_custom_call" | custom-call | flops 17179869184 | bytes 4194304 | tf_op jit(solution)/shard_map/pallas_call | solution.py:257
  146.9 5.2 %all-to-all-start.2 = ((bf16[32,128,128]{2,1,0:T(8,128)(2,1)}), bf16[32,128,128]{2,1,0:T(8,128)(2,1)S(1)}, u32[]{:S(2)}, u32[]{:S(2)}) async-start(bf16[32,128,128]{2,1,0:T(8,128)(2,1)} %shard_map.67), calls=%async_computation.2 | async-start | bytes 2097152 | tf_op jit(solution)/shard_map/all_to_all | solution.py:33
  152.3 1.9 collective-permute-done.14
  155.4 2.4 %collective-permute-start.16 = (bf16[256,2048]{1,0:T(8,128)(2,1)S(1)}, bf16[256,2048]{1,0:T(8,128)(2,1)S(1)}, u32[]{:S(2)}, u32[]{:S(2)}) collective-permute-start(bf16[256,2048]{1,0:T(8,128)(2,1)S(1)} %maximum_select_fusion.w0), channel_id=1, source_target_pairs={{0,6},{2,0},{4,2},{6,4},{1,7},{3,1},{5,3},{7,5},{8,14},{10,8},{12,... | collective-permute-start | bytes 3145736 | tf_op jit(solution)/shard_map/ppermute | solution.py:25
  157.8 23.8 %collective-permute-done.15.w1 = bf16[256,2048]{1,0:T(8,128)(2,1)S(1)} collective-permute-done((bf16[256,2048]{1,0:T(8,128)(2,1)S(1)}, bf16[256,2048]{1,0:T(8,128)(2,1)S(1)}, u32[]{:S(2)}, u32[]{:S(2)}) %collective-permute-start.15) | collective-permute-done | bytes 1048608 | tf_op jit(solution)/shard_map/ppermute | solution.py:25
  181.7 21.0 %collective-permute-done.16.w2 = bf16[256,2048]{1,0:T(8,128)(2,1)S(1)} collective-permute-done((bf16[256,2048]{1,0:T(8,128)(2,1)S(1)}, bf16[256,2048]{1,0:T(8,128)(2,1)S(1)}, u32[]{:S(2)}, u32[]{:S(2)}) %collective-permute-start.16) | collective-permute-done | bytes 1048608 | tf_op jit(solution)/shard_map/ppermute | solution.py:25
  207.1 2.9 %shard_map.69 = bf16[256,2048]{1,0:T(8,128)(2,1)S(1)} custom-call(s32[3]{0:T(128)S(1)} %pad_add_fusion.where_ref, bf16[32,128,128]{2,1,0:T(8,128)(2,1)S(1)} %all-to-all-done.2.back, bf16[256,2048]{1,0:T(8,128)(2,1)S(1)} %maximum_select_fusion.w0, bf16[256,2048]{1,0:T(8,128)(2,1)S(1)} %collective-permute-done.15.w1, bf16[256,2048]{1,0:T(8,128)(2,1)S(1)} %copy-done.1, ...), custom_call_target="tpu_custom_call" | custom-call | flops 1073741824 | bytes 4194304 | tf_op jit(solution)/shard_map/pallas_call | solution.py:297
  210.1 3.0 %shard_map.68 = f32[256,2048]{1,0:T(8,128)S(1)} custom-call(s32[3]{0:T(128)S(1)} %pad_add_fusion.where_ref, bf16[32,128,128]{2,1,0:T(8,128)(2,1)S(1)} %all-to-all-done.2.back, bf16[256,2048]{1,0:T(8,128)(2,1)S(1)} %maximum_select_fusion.w0, bf16[256,2048]{1,0:T(8,128)(2,1)S(1)} %collective-permute-done.15.w1, bf16[256,2048]{1,0:T(8,128)(2,1)S(1)} %copy-done.1, ...), custom_call_target="tpu_custom_call" | custom-call | flops 1073741824 | bytes 4194304 | tf_op jit(solution)/shard_map/pallas_call | solution.py:297
  (55 shorter events, 19.1 us)
Async XLA Ops:
  0.0 6.1 %copy-start.4 = (bf16[2,128,2048]{2,1,0:T(8,128)(2,1)S(1)}, bf16[2,128,2048]{2,1,0:T(8,128)(2,1)}, u32[]{:S(2)}) copy-start(bf16[2,128,2048]{2,1,0:T(8,128)(2,1)} %param.6) | copy-start | bytes 3145732
  0.0 8.3 %copy-start.7 = (f32[2,128,32]{1,2,0:T(8,128)S(1)}, f32[2,128,32]{1,2,0:T(8,128)}, u32[]{:S(2)}) copy-start(f32[2,128,32]{1,2,0:T(8,128)} %param.7) | copy-start | bytes 98308
  1.2 1.6 collective-permute-start.4
  1.3 22.2 %collective-permute-start = (bf16[256,2048]{1,0:T(8,128)(2,1)}, bf16[256,2048]{1,0:T(8,128)(2,1)}, u32[]{:S(2)}, u32[]{:S(2)}) collective-permute-start(bf16[256,2048]{1,0:T(8,128)(2,1)} %bitcast.13), channel_id=1, source_target_pairs={{0,1},{1,0},{2,3},{3,2},{4,5},{5,4},{6,7},{7,6},{8,9},{9,8},{10,11... | collective-permute-start | bytes 3145736 | tf_op jit(solution)/shard_map/ppermute | solution.py:29
  2.8 15.3 %collective-permute-start.5 = (bf16[512,512]{1,0:T(8,128)(2,1)S(1)}, bf16[512,512]{1,0:T(8,128)(2,1)S(1)}, u32[]{:S(2)}, u32[]{:S(2)}) collective-permute-start(bf16[512,512]{1,0:T(8,128)(2,1)S(1)} %pad_maximum_fusion.1.w0), channel_id=1, source_target_pairs={{0,2},{2,4},{4,6},{6,0},{1,3},{3,5},{5,7},{7,1},{8,10},{10,12},{12... | collective-permute-start | bytes 1572872 | tf_op jit(solution)/shard_map/ppermute | solution.py:25
  4.4 14.1 %collective-permute-start.6 = (bf16[512,512]{1,0:T(8,128)(2,1)S(1)}, bf16[512,512]{1,0:T(8,128)(2,1)S(1)}, u32[]{:S(2)}, u32[]{:S(2)}) collective-permute-start(bf16[512,512]{1,0:T(8,128)(2,1)S(1)} %pad_maximum_fusion.1.w0), channel_id=1, source_target_pairs={{0,6},{2,0},{4,2},{6,4},{1,7},{3,1},{5,3},{7,5},{8,14},{10,8},{12,... | collective-permute-start | bytes 1572872 | tf_op jit(solution)/shard_map/ppermute | solution.py:25
  6.1 36.3 %collective-permute-start.1 = (bf16[256,2048]{1,0:T(8,128)(2,1)S(1)}, bf16[256,2048]{1,0:T(8,128)(2,1)}, u32[]{:S(2)}, u32[]{:S(2)}) collective-permute-start(bf16[256,2048]{1,0:T(8,128)(2,1)S(1)} %bitcast.14), channel_id=1, source_target_pairs={{0,8},{8,0},{1,9},{9,1},{2,10},{10,2},{3,11},{11,3},{4,12},{12,4},... | collective-permute-start | bytes 3145736 | tf_op jit(solution)/shard_map/ppermute | solution.py:29
  18.1 8.8 %collective-permute-start.11 = (bf16[256,512]{1,0:T(8,128)(2,1)S(1)}, bf16[256,512]{1,0:T(8,128)(2,1)S(1)}, u32[]{:S(2)}, u32[]{:S(2)}) collective-permute-start(bf16[256,512]{1,0:T(8,128)(2,1)S(1)} %slice.36), channel_id=1, source_target_pairs={{0,2},{2,4},{4,6},{6,0},{1,3},{3,5},{5,7},{7,1},{8,10},{10,12},{12... | collective-permute-start | bytes 786440 | tf_op jit(solution)/shard_map/ppermute | solution.py:25
  19.2 8.0 %collective-permute-start.12 = (bf16[256,512]{1,0:T(8,128)(2,1)}, bf16[256,512]{1,0:T(8,128)(2,1)S(1)}, u32[]{:S(2)}, u32[]{:S(2)}) collective-permute-start(bf16[256,512]{1,0:T(8,128)(2,1)} %slice.37), channel_id=1, source_target_pairs={{0,6},{2,0},{4,2},{6,4},{1,7},{3,1},{5,3},{7,5},{8,14},{10,8},{12,... | collective-permute-start | bytes 786440 | tf_op jit(solution)/shard_map/ppermute | solution.py:25
  22.2 1.3 collective-permute-start.10
  30.7 49.1 %all-to-all-start.1 = ((bf16[32,80,128]{2,1,0:T(8,128)(2,1)}), bf16[32,80,128]{2,1,0:T(8,128)(2,1)S(1)}, u32[]{:S(2)}, u32[]{:S(2)}) async-start(bf16[32,80,128]{2,1,0:T(8,128)(2,1)} %shard_map.66), calls=%async_computation.1 | async-start | bytes 1310720 | tf_op jit(solution)/shard_map/all_to_all | solution.py:33
  42.4 32.3 %collective-permute-start.2 = (bf16[256,2048]{1,0:T(8,128)(2,1)}, bf16[256,2048]{1,0:T(8,128)(2,1)S(1)}, u32[]{:S(2)}, u32[]{:S(2)}) collective-permute-start(bf16[256,2048]{1,0:T(8,128)(2,1)} %collective-permute-done.1.t2), channel_id=1, source_target_pairs={{0,1},{1,0},{2,3},{3,2},{4,5},{5,4},{6,7},{7,6},{8,9},{9,8},{10,11... | collective-permute-start | bytes 3145736 | tf_op jit(solution)/shard_map/ppermute | solution.py:29
  44.4 1.7 collective-permute-start.3
  46.2 16.1 %collective-permute-start.7 = (bf16[512,512]{1,0:T(8,128)(2,1)S(1)}, bf16[512,512]{1,0:T(8,128)(2,1)S(1)}, u32[]{:S(2)}, u32[]{:S(2)}) collective-permute-start(bf16[512,512]{1,0:T(8,128)(2,1)S(1)} %pad_maximum_fusion.w0), channel_id=1, source_target_pairs={{0,2},{2,4},{4,6},{6,0},{1,3},{3,5},{5,7},{7,1},{8,10},{10,12},{12... | collective-permute-start | bytes 1572872 | tf_op jit(solution)/shard_map/ppermute | solution.py:25
  47.3 25.6 %collective-permute-start.8 = (bf16[512,512]{1,0:T(8,128)(2,1)S(1)}, bf16[512,512]{1,0:T(8,128)(2,1)S(1)}, u32[]{:S(2)}, u32[]{:S(2)}) collective-permute-start(bf16[512,512]{1,0:T(8,128)(2,1)S(1)} %pad_maximum_fusion.w0), channel_id=1, source_target_pairs={{0,6},{2,0},{4,2},{6,4},{1,7},{3,1},{5,3},{7,5},{8,14},{10,8},{12,... | collective-permute-start | bytes 1572872 | tf_op jit(solution)/shard_map/ppermute | solution.py:25
  50.0 24.8 %collective-permute-start.9 = (bf16[512,512]{1,0:T(8,128)(2,1)S(1)}, bf16[512,512]{1,0:T(8,128)(2,1)S(1)}, u32[]{:S(2)}, u32[]{:S(2)}) collective-permute-start(bf16[512,512]{1,0:T(8,128)(2,1)S(1)} %pad_maximum_fusion.w0), channel_id=1, source_target_pairs={{0,4},{2,6},{4,0},{6,2},{1,5},{3,7},{5,1},{7,3},{8,12},{10,14},{12... | collective-permute-start | bytes 1572872 | tf_op jit(solution)/shard_map/ppermute | solution.py:25
  79.8 38.1 %all-to-all-start = ((bf16[16,128,256]{2,1,0:T(8,128)(2,1)}), bf16[16,128,256]{2,1,0:T(8,128)(2,1)S(1)}, u32[]{:S(2)}, u32[]{:S(2)}) async-start(bf16[16,128,256]{2,1,0:T(8,128)(2,1)} %shard_map.65), calls=%async_computation | async-start | bytes 2097152 | tf_op jit(solution)/shard_map/all_to_all | solution.py:33
  88.1 2.0 collective-permute-start.13
  146.9 57.7 %all-to-all-start.2 = ((bf16[32,128,128]{2,1,0:T(8,128)(2,1)}), bf16[32,128,128]{2,1,0:T(8,128)(2,1)S(1)}, u32[]{:S(2)}, u32[]{:S(2)}) async-start(bf16[32,128,128]{2,1,0:T(8,128)(2,1)} %shard_map.67), calls=%async_computation.2 | async-start | bytes 2097152 | tf_op jit(solution)/shard_map/all_to_all | solution.py:33
  152.2 2.0 collective-permute-start.14
  154.4 27.2 %collective-permute-start.15 = (bf16[256,2048]{1,0:T(8,128)(2,1)S(1)}, bf16[256,2048]{1,0:T(8,128)(2,1)S(1)}, u32[]{:S(2)}, u32[]{:S(2)}) collective-permute-start(bf16[256,2048]{1,0:T(8,128)(2,1)S(1)} %maximum_select_fusion.w0), channel_id=1, source_target_pairs={{0,2},{2,4},{4,6},{6,0},{1,3},{3,5},{5,7},{7,1},{8,10},{10,12},{12... | collective-permute-start | bytes 3145736 | tf_op jit(solution)/shard_map/ppermute | solution.py:25
  155.4 47.3 %collective-permute-start.16 = (bf16[256,2048]{1,0:T(8,128)(2,1)S(1)}, bf16[256,2048]{1,0:T(8,128)(2,1)S(1)}, u32[]{:S(2)}, u32[]{:S(2)}) collective-permute-start(bf16[256,2048]{1,0:T(8,128)(2,1)S(1)} %maximum_select_fusion.w0), channel_id=1, source_target_pairs={{0,6},{2,0},{4,2},{6,4},{1,7},{3,1},{5,3},{7,5},{8,14},{10,8},{12,... | collective-permute-start | bytes 3145736 | tf_op jit(solution)/shard_map/ppermute | solution.py:25
  157.7 45.9 %collective-permute-start.17 = (bf16[256,2048]{1,0:T(8,128)(2,1)S(1)}, bf16[256,2048]{1,0:T(8,128)(2,1)S(1)}, u32[]{:S(2)}, u32[]{:S(2)}) collective-permute-start(bf16[256,2048]{1,0:T(8,128)(2,1)S(1)} %maximum_select_fusion.w0), channel_id=1, source_target_pairs={{0,4},{2,6},{4,0},{6,2},{1,5},{3,7},{5,1},{7,3},{8,12},{10,14},{12... | collective-permute-start | bytes 3145736 | tf_op jit(solution)/shard_map/ppermute | solution.py:25
  210.0 3.1 %collective-permute-start.18 = (bf16[256,2048]{1,0:T(8,128)(2,1)S(1)}, bf16[256,2048]{1,0:T(8,128)(2,1)S(1)}, u32[]{:S(2)}, u32[]{:S(2)}) collective-permute-start(bf16[256,2048]{1,0:T(8,128)(2,1)S(1)} %shard_map.69), channel_id=1, source_target_pairs={{0,1},{1,0},{2,3},{3,2},{4,5},{5,4},{6,7},{7,6},{8,9},{9,8},{10,11... | collective-permute-start | bytes 3145736 | tf_op jit(solution)/shard_map/ppermute | solution.py:29
  (6 other events, 10.8 us)

commit v2 on v1

--- a/solution.py
+++ b/solution.py
@@ -14,7 +14,7 @@
 BLOCKS = 32
 UNITS = 16
 LENGTH = BLOCKS * POS
-TILE = 512
+TILE = 1024
 PART = 256
 NEG = -1e30
 VMEM = pl.BlockSpec(memory_space=pltpu.VMEM)
@@ -181,18 +181,21 @@
             query[h, 64:128, at] = ones
 
     def score(h, i, j, slot, diagonal, r):
+        rows = slice(r * PART, r * PART + PART)
+        skip = r * PART if diagonal else 0
         s = jnp.dot(
             keys[pl.ds(pl.multiple_of(j * TILE + r * PART, PART), PART), :],
-            query[h, :, pl.ds(pl.multiple_of(i * TILE, TILE), TILE)],
+            query[h, :, pl.ds(pl.multiple_of(i * TILE + skip, PART), TILE - skip)],
             preferred_element_type=jnp.float32,
         )
         if diagonal:
-            a = lax.broadcasted_iota(jnp.int32, (PART, TILE), 0)
-            b = lax.broadcasted_iota(jnp.int32, (PART, TILE), 1)
-            s = jnp.where(a + r * PART <= b, s, NEG)
-        scores[slot, r * PART : r * PART + PART] = s
+            a = lax.broadcasted_iota(jnp.int32, (PART, PART), 0)
+            b = lax.broadcasted_iota(jnp.int32, (PART, PART), 1)
+            near = jnp.where(a <= b, s[:, :PART], NEG)
+            s = near if skip + PART == TILE else jnp.concatenate([near, s[:, PART:]], axis=1)
+        scores[slot, rows, skip:] = s
         m = jnp.max(s, axis=0, keepdims=True)
-        peak[slot] = m if r == 0 else jnp.maximum(peak[slot], m)
+        peak[slot, :, skip:] = m if r == 0 else jnp.maximum(peak[slot, :, skip:], m)
 
     def begin(j, slot):
         before = jnp.where(j == 0, NEG, top[...])
@@ -200,9 +203,11 @@
         top[...] = now
         total[...] = total[...] * jnp.exp(before - now)
 
-    def add(j, slot, r):
-        p = jnp.exp(scores[slot, r * PART : r * PART + PART] - top[...]).astype(jnp.bfloat16)
-        total[...] += jnp.dot(
+    def add(j, slot, r, diagonal):
+        skip = r * PART if diagonal else 0
+        rows = slice(r * PART, r * PART + PART)
+        p = jnp.exp(scores[slot, rows, skip:] - top[:, skip:]).astype(jnp.bfloat16)
+        total[:, skip:] += jnp.dot(
             values[:, pl.ds(pl.multiple_of(j * TILE + r * PART, PART), PART)], p,
             preferred_element_type=jnp.float32,
         )
@@ -226,19 +231,29 @@
         later_j = jnp.where(last, 0, j + 1)
         safe_h = jnp.minimum(later_h, 1)
 
-        def go(diagonal):
+        def go(diagonal, here):
             begin(j, slot)
             for r in range(TILE // PART):
                 score(safe_h, later_i, later_j, 1 - slot, diagonal, r)
-                add(j, slot, r)
-
-        @pl.when(later_i == later_j)
-        def _():
-            go(True)
-
-        @pl.when(later_i != later_j)
-        def _():
-            go(False)
+                add(j, slot, r, here)
+
+        later = later_i == later_j
+
+        @pl.when(later & last)
+        def _():
+            go(True, True)
+
+        @pl.when(later & jnp.logical_not(last))
+        def _():
+            go(True, False)
+
+        @pl.when(jnp.logical_not(later) & last)
+        def _():
+            go(False, True)
+
+        @pl.when(jnp.logical_not(later | last))
+        def _():
+            go(False, False)
 
         @pl.when(last)
         def _():
@@ -255,8 +270,8 @@
 
 def attend(where, query, mine, theirs):
     return call(
-        attend_kernel, 4 * LENGTH * LENGTH * 256,
-        out_shape=jax.ShapeDtypeStruct((BLOCKS, 128, POS), jnp.bfloat16),
+        attend_kernel, 4 * LENGTH * LENGTH * 256, 32,
+        out_shape=pltpu.HBM((BLOCKS, 128, POS), jnp.bfloat16),
         in_specs=[SMEM] + [VMEM] * 3, out_specs=VMEM,
         scratch_shapes=[
             pltpu.VMEM((LENGTH, 128), jnp.bfloat16),
@@ -270,36 +285,33 @@
     )(where, query, mine, theirs)
 
 
-def mix_kernel(own, where_ref, back, w0, w1, w2, w3, out_ref, left):
+def mix_kernel(own, where_ref, back, w0, w1, w2, w3, out_ref):
     x = where_ref[0]
     c = where_ref[1]
     base = 2 * (c if own else 1 - c)
-
-    @pl.when(pl.program_id(0) == 0)
-    def _():
-        for k, step in enumerate((0, 3, 1, 2)):
-            chip = lax.rem(x + step, X)
-            for s in range(2):
-                unit = (base + s) * GROUPS + lax.rem(chip, 2) * 4 + lax.div(chip, 2)
-                block = jnp.concatenate([back[unit], back[unit + 2]], axis=0)
-                block = block.astype(jnp.float32).T.astype(jnp.bfloat16)
-                left[k, s * POS : s * POS + POS] = block
-
-    total = None
-    for k, ref in enumerate((w0, w1, w2, w3)):
-        part = jnp.dot(left[k], ref[...], preferred_element_type=jnp.float32)
-        total = part if total is None else total + part
-    out_ref[...] = total.astype(out_ref.dtype)
+    left = []
+    for step in (0, 3, 1, 2):
+        chip = lax.rem(x + step, X)
+        rows = []
+        for s in range(2):
+            unit = (base + s) * GROUPS + lax.rem(chip, 2) * 4 + lax.div(chip, 2)
+            block = jnp.concatenate([back[unit], back[unit + 2]], axis=0)
+            rows.append(block.astype(jnp.float32).T.astype(jnp.bfloat16))
+        left.append(jnp.concatenate(rows, axis=0))
+    for n in range(8):
+        at = slice(n * 256, n * 256 + 256)
+        total = None
+        for a, ref in zip(left, (w0, w1, w2, w3)):
+            part = jnp.dot(a, ref[:, at], preferred_element_type=jnp.float32)
+            total = part if total is None else total + part
+        out_ref[:, at] = total.astype(out_ref.dtype)
 
 
 def mix(own, where, back, weights):
-    part = pl.BlockSpec((256, 512), lambda n: (0, n))
     return call(
         functools.partial(mix_kernel, own), 2 * 256 * 1024 * 2048,
-        grid=(4,),
         out_shape=jax.ShapeDtypeStruct((256, 2048), jnp.float32 if own else jnp.bfloat16),
-        in_specs=[SMEM, VMEM] + [part] * 4, out_specs=part,
-        scratch_shapes=[pltpu.VMEM((4, 256, 256), jnp.bfloat16)],
+        in_specs=[SMEM] + [VMEM] * 5, out_specs=VMEM,
     )(where, back, *weights)
 
 

time: 216 us -> 208 us (0.963)
  Pallas kernels: 44.2 us -> 35.3 us
    pallas_call x3, Pallas kernels: 35 us -> 26.2 us  [the longest x1 22.4 us: attend(): call(attend_kernel, 4 * LENGTH * LENGTH * 256, 32, out_shape=pltpu.HBM((B...]
  transfers between devices with their start and end apart: 22 -> 22, of which waited for: 14 -> 15; matrix products, arithmetic and copies ran while one was open for 1% -> 1% of each run, Pallas kernels for 6% -> 5%
where the time goes in v2:
time: 208 us; the launch traced here: 206 us
  waiting for transfers between devices  117 us (56%)
  starting transfers between devices  44.3 us (21%)
  Pallas kernels  35.3 us (17%)
  local copies, waits for them, and re-layouts  6.42 us (3%)
  other arithmetic  2.92 us (1%)
    ppermute x10, waiting for transfers between devices, shift(): return lax.ppermute(value, 'x', [(i, (i + by) % X) for i in range(X)])  81.7 us
    all_to_all x3, waiting for transfers between devices, exchange(): return lax.all_to_all(value, axes, 0, 0, tiled=True)  27.7 us
    all_to_all x3, starting transfers between devices, exchange(): return lax.all_to_all(value, axes, 0, 0, tiled=True)  25.1 us
    pallas_call x1, Pallas kernels, attend(): call(attend_kernel, 4 * LENGTH * LENGTH * 256, 32, out_shape=pltpu.HBM((B...  22.4 us
    ppermute x10, starting transfers between devices, shift(): return lax.ppermute(value, 'x', [(i, (i + by) % X) for i in range(X)])  15.4 us
    ppermute x9, waiting for transfers between devices, swap(): return lax.ppermute(value, axis, [(0, 1), (1, 0)])  7.85 us
    unnamed x16, local copies, waits for them, and re-layouts  5.61 us
    pallas_call x1, Pallas kernels, project_q(): call(project_q_kernel, 2 * 1024 * 2048 * 512, out_shape=jax.ShapeDtypeStr...  5 us
  transfers between devices with their start and end apart: 22, of which 15 were waited for; matrix products, arithmetic and copies ran while one was open for 1% of the time, Pallas kernels for 5%

profile of v2, /device:TPU:8, one launch (start us, length us, event | category | flops | bytes accessed | tf_op | source)
XLA Modules:
  0.0 206.5 jit_solution(17961152414780400917)
XLA Ops:
  2.8 1.6 collective-permute-start.5
  4.4 1.7 collective-permute-start.6
  6.1 2.2 %collective-permute-start.1 = (bf16[256,2048]{1,0:T(8,128)(2,1)S(1)}, bf16[256,2048]{1,0:T(8,128)(2,1)}, u32[]{:S(2)}, u32[]{:S(2)}) collective-permute-start(bf16[256,2048]{1,0:T(8,128)(2,1)S(1)} %bitcast.14), channel_id=1, source_target_pairs={{0,8},{8,0},{1,9},{9,1},{2,10},{10,2},{3,11},{11,3},{4,12},{12,4},... | collective-permute-start | bytes 3145736 | tf_op jit(solution)/shard_map/ppermute | solution.py:29
  8.3 9.8 %collective-permute-done.5.w1 = bf16[512,512]{1,0:T(8,128)(2,1)S(1)} collective-permute-done((bf16[512,512]{1,0:T(8,128)(2,1)S(1)}, bf16[512,512]{1,0:T(8,128)(2,1)S(1)}, u32[]{:S(2)}, u32[]{:S(2)}) %collective-permute-start.5) | collective-permute-done | bytes 524320 | tf_op jit(solution)/shard_map/ppermute | solution.py:25
  19.2 3.0 %collective-permute-start.12 = (bf16[256,512]{1,0:T(8,128)(2,1)}, bf16[256,512]{1,0:T(8,128)(2,1)S(1)}, u32[]{:S(2)}, u32[]{:S(2)}) collective-permute-start(bf16[256,512]{1,0:T(8,128)(2,1)} %slice.37), channel_id=1, source_target_pairs={{0,6},{2,0},{4,2},{6,4},{1,7},{3,1},{5,3},{7,5},{8,14},{10,8},{12,... | collective-permute-start | bytes 786440 | tf_op jit(solution)/shard_map/ppermute | solution.py:25
  23.5 3.4 %collective-permute-done.11.w3 = bf16[256,512]{1,0:T(8,128)(2,1)S(1)} collective-permute-done((bf16[256,512]{1,0:T(8,128)(2,1)S(1)}, bf16[256,512]{1,0:T(8,128)(2,1)S(1)}, u32[]{:S(2)}, u32[]{:S(2)}) %collective-permute-start.11) | collective-permute-done | bytes 262176 | tf_op jit(solution)/shard_map/ppermute | solution.py:25
  27.2 3.5 %shard_map.66 = bf16[32,80,128]{2,1,0:T(8,128)(2,1)} custom-call(s32[3]{0:T(128)S(1)} %pad_add_fusion.where_ref, bf16[256,2048]{1,0:T(8,128)(2,1)S(1)} %bitcast.15, bf16[256,2048]{1,0:T(8,128)(2,1)} %collective-permute-done.t1, f32[32,2,128]{2,1,0:T(2,128)S(1)} %bitcast.17, bf16[512,512]{1,0:T(8,128)(2,1)S(1)} %pad_maximum_fusion.1.w0, ...), custom_call_target="tpu_custom_call" | custom-call | flops 1073741824 | bytes 4194304 | tf_op jit(solution)/shard_map/pallas_call | solution.py:126
  30.7 11.7 %all-to-all-start.1 = ((bf16[32,80,128]{2,1,0:T(8,128)(2,1)}), bf16[32,80,128]{2,1,0:T(8,128)(2,1)S(1)}, u32[]{:S(2)}, u32[]{:S(2)}) async-start(bf16[32,80,128]{2,1,0:T(8,128)(2,1)} %shard_map.66), calls=%async_computation.1 | async-start | bytes 1310720 | tf_op jit(solution)/shard_map/all_to_all | solution.py:33
  47.3 2.7 %collective-permute-start.8 = (bf16[512,512]{1,0:T(8,128)(2,1)S(1)}, bf16[512,512]{1,0:T(8,128)(2,1)S(1)}, u32[]{:S(2)}, u32[]{:S(2)}) collective-permute-start(bf16[512,512]{1,0:T(8,128)(2,1)S(1)} %pad_maximum_fusion.w0), channel_id=1, source_target_pairs={{0,6},{2,0},{4,2},{6,4},{1,7},{3,1},{5,3},{7,5},{8,14},{10,8},{12,... | collective-permute-start | bytes 1572872 | tf_op jit(solution)/shard_map/ppermute | solution.py:25
  51.3 11.0 %collective-permute-done.7.w1 = bf16[512,512]{1,0:T(8,128)(2,1)S(1)} collective-permute-done((bf16[512,512]{1,0:T(8,128)(2,1)S(1)}, bf16[512,512]{1,0:T(8,128)(2,1)S(1)}, u32[]{:S(2)}, u32[]{:S(2)}) %collective-permute-start.7) | collective-permute-done | bytes 524320 | tf_op jit(solution)/shard_map/ppermute | solution.py:25
  62.3 10.6 %collective-permute-done.8.w2 = bf16[512,512]{1,0:T(8,128)(2,1)S(1)} collective-permute-done((bf16[512,512]{1,0:T(8,128)(2,1)S(1)}, bf16[512,512]{1,0:T(8,128)(2,1)S(1)}, u32[]{:S(2)}, u32[]{:S(2)}) %collective-permute-start.8) | collective-permute-done | bytes 524320 | tf_op jit(solution)/shard_map/ppermute | solution.py:25
  72.9 1.8 collective-permute-done.9.w3
  74.7 5.0 %shard_map.65 = bf16[16,128,256]{2,1,0:T(8,128)(2,1)} custom-call(s32[3]{0:T(128)S(1)} %pad_add_fusion.where_ref, bf16[256,2048]{1,0:T(8,128)(2,1)S(1)} %bitcast.16, bf16[256,2048]{1,0:T(8,128)(2,1)} %collective-permute-done.t1, bf16[256,2048]{1,0:T(8,128)(2,1)} %collective-permute-done.1.t2, bf16[256,2048]{1,0:T(8,128)(2,1)S(1)} %collective-permute-done.2.t3, ...), custom_call_target="tpu_custom_call" | custom-call | flops 2147483648 | bytes 4194304 | tf_op jit(solution)/shard_map/pallas_call | solution.py:149
  79.7 8.3 %all-to-all-start = ((bf16[16,128,256]{2,1,0:T(8,128)(2,1)}), bf16[16,128,256]{2,1,0:T(8,128)(2,1)S(1)}, u32[]{:S(2)}, u32[]{:S(2)}) async-start(bf16[16,128,256]{2,1,0:T(8,128)(2,1)} %shard_map.65), calls=%async_computation | async-start | bytes 2097152 | tf_op jit(solution)/shard_map/all_to_all | solution.py:33
  88.2 1.9 collective-permute-done.13.theirs_ref
  90.1 27.7 %all-to-all-done.q_ref = bf16[16,128,256]{2,1,0:T(8,128)(2,1)S(1)} async-done(((bf16[16,128,256]{2,1,0:T(8,128)(2,1)}), bf16[16,128,256]{2,1,0:T(8,128)(2,1)S(1)}, u32[]{:S(2)}, u32[]{:S(2)}) %all-to-all-start) | async-done | bytes 1048608 | tf_op jit(solution)/shard_map/all_to_all | solution.py:33
  117.8 22.4 %shard_map.67 = bf16[32,128,128]{2,1,0:T(8,128)(2,1)} custom-call(s32[3]{0:T(128)S(1)} %pad_add_fusion.where_ref, bf16[16,128,256]{2,1,0:T(8,128)(2,1)S(1)} %all-to-all-done.q_ref, bf16[32,80,128]{2,1,0:T(8,128)(2,1)S(1)} %all-to-all-done.1.mine_ref, bf16[32,64,128]{2,1,0:T(8,128)(2,1)S(1)} %collective-permute-done.13.theirs_ref), custom_call_target="tpu_custom_call" | custom-call | flops 17179869184 | bytes 4194304 | tf_op jit(solution)/shard_map/pallas_call | solution.py:272
  140.2 5.2 %all-to-all-start.2 = ((bf16[32,128,128]{2,1,0:T(8,128)(2,1)}), bf16[32,128,128]{2,1,0:T(8,128)(2,1)S(1)}, u32[]{:S(2)}, u32[]{:S(2)}) async-start(bf16[32,128,128]{2,1,0:T(8,128)(2,1)} %shard_map.67), calls=%async_computation.2 | async-start | bytes 2097152 | tf_op jit(solution)/shard_map/all_to_all | solution.py:33
  145.6 1.9 collective-permute-done.14
  148.9 2.4 %collective-permute-start.16 = (bf16[256,2048]{1,0:T(8,128)(2,1)S(1)}, bf16[256,2048]{1,0:T(8,128)(2,1)S(1)}, u32[]{:S(2)}, u32[]{:S(2)}) collective-permute-start(bf16[256,2048]{1,0:T(8,128)(2,1)S(1)} %maximum_select_fusion.w0), channel_id=1, source_target_pairs={{0,6},{2,0},{4,2},{6,4},{1,7},{3,1},{5,3},{7,5},{8,14},{10,8},{12,... | collective-permute-start | bytes 3145736 | tf_op jit(solution)/shard_map/ppermute | solution.py:25
  151.4 23.8 %collective-permute-done.15.w1 = bf16[256,2048]{1,0:T(8,128)(2,1)S(1)} collective-permute-done((bf16[256,2048]{1,0:T(8,128)(2,1)S(1)}, bf16[256,2048]{1,0:T(8,128)(2,1)S(1)}, u32[]{:S(2)}, u32[]{:S(2)}) %collective-permute-start.15) | collective-permute-done | bytes 1048608 | tf_op jit(solution)/shard_map/ppermute | solution.py:25
  175.2 21.0 %collective-permute-done.16.w2 = bf16[256,2048]{1,0:T(8,128)(2,1)S(1)} collective-permute-done((bf16[256,2048]{1,0:T(8,128)(2,1)S(1)}, bf16[256,2048]{1,0:T(8,128)(2,1)S(1)}, u32[]{:S(2)}, u32[]{:S(2)}) %collective-permute-start.16) | collective-permute-done | bytes 1048608 | tf_op jit(solution)/shard_map/ppermute | solution.py:25
  200.6 1.9 shard_map.69
  202.6 1.9 shard_map.68
  (55 shorter events, 20.1 us)
Async XLA Ops:
  0.0 6.1 %copy-start.4 = (bf16[2,128,2048]{2,1,0:T(8,128)(2,1)S(1)}, bf16[2,128,2048]{2,1,0:T(8,128)(2,1)}, u32[]{:S(2)}) copy-start(bf16[2,128,2048]{2,1,0:T(8,128)(2,1)} %param.6) | copy-start | bytes 3145732
  0.0 8.3 %copy-start.7 = (f32[2,128,32]{1,2,0:T(8,128)S(1)}, f32[2,128,32]{1,2,0:T(8,128)}, u32[]{:S(2)}) copy-start(f32[2,128,32]{1,2,0:T(8,128)} %param.7) | copy-start | bytes 98308
  1.2 1.6 collective-permute-start.4
  1.3 22.2 %collective-permute-start = (bf16[256,2048]{1,0:T(8,128)(2,1)}, bf16[256,2048]{1,0:T(8,128)(2,1)}, u32[]{:S(2)}, u32[]{:S(2)}) collective-permute-start(bf16[256,2048]{1,0:T(8,128)(2,1)} %bitcast.13), channel_id=1, source_target_pairs={{0,1},{1,0},{2,3},{3,2},{4,5},{5,4},{6,7},{7,6},{8,9},{9,8},{10,11... | collective-permute-start | bytes 3145736 | tf_op jit(solution)/shard_map/ppermute | solution.py:29
  2.8 15.3 %collective-permute-start.5 = (bf16[512,512]{1,0:T(8,128)(2,1)S(1)}, bf16[512,512]{1,0:T(8,128)(2,1)S(1)}, u32[]{:S(2)}, u32[]{:S(2)}) collective-permute-start(bf16[512,512]{1,0:T(8,128)(2,1)S(1)} %pad_maximum_fusion.1.w0), channel_id=1, source_target_pairs={{0,2},{2,4},{4,6},{6,0},{1,3},{3,5},{5,7},{7,1},{8,10},{10,12},{12... | collective-permute-start | bytes 1572872 | tf_op jit(solution)/shard_map/ppermute | solution.py:25
  4.4 14.1 %collective-permute-start.6 = (bf16[512,512]{1,0:T(8,128)(2,1)S(1)}, bf16[512,512]{1,0:T(8,128)(2,1)S(1)}, u32[]{:S(2)}, u32[]{:S(2)}) collective-permute-start(bf16[512,512]{1,0:T(8,128)(2,1)S(1)} %pad_maximum_fusion.1.w0), channel_id=1, source_target_pairs={{0,6},{2,0},{4,2},{6,4},{1,7},{3,1},{5,3},{7,5},{8,14},{10,8},{12,... | collective-permute-start | bytes 1572872 | tf_op jit(solution)/shard_map/ppermute | solution.py:25
  6.1 36.3 %collective-permute-start.1 = (bf16[256,2048]{1,0:T(8,128)(2,1)S(1)}, bf16[256,2048]{1,0:T(8,128)(2,1)}, u32[]{:S(2)}, u32[]{:S(2)}) collective-permute-start(bf16[256,2048]{1,0:T(8,128)(2,1)S(1)} %bitcast.14), channel_id=1, source_target_pairs={{0,8},{8,0},{1,9},{9,1},{2,10},{10,2},{3,11},{11,3},{4,12},{12,4},... | collective-permute-start | bytes 3145736 | tf_op jit(solution)/shard_map/ppermute | solution.py:29
  18.1 8.8 %collective-permute-start.11 = (bf16[256,512]{1,0:T(8,128)(2,1)S(1)}, bf16[256,512]{1,0:T(8,128)(2,1)S(1)}, u32[]{:S(2)}, u32[]{:S(2)}) collective-permute-start(bf16[256,512]{1,0:T(8,128)(2,1)S(1)} %slice.36), channel_id=1, source_target_pairs={{0,2},{2,4},{4,6},{6,0},{1,3},{3,5},{5,7},{7,1},{8,10},{10,12},{12... | collective-permute-start | bytes 786440 | tf_op jit(solution)/shard_map/ppermute | solution.py:25
  19.2 8.0 %collective-permute-start.12 = (bf16[256,512]{1,0:T(8,128)(2,1)}, bf16[256,512]{1,0:T(8,128)(2,1)S(1)}, u32[]{:S(2)}, u32[]{:S(2)}) collective-permute-start(bf16[256,512]{1,0:T(8,128)(2,1)} %slice.37), channel_id=1, source_target_pairs={{0,6},{2,0},{4,2},{6,4},{1,7},{3,1},{5,3},{7,5},{8,14},{10,8},{12,... | collective-permute-start | bytes 786440 | tf_op jit(solution)/shard_map/ppermute | solution.py:25
  22.2 1.3 collective-permute-start.10
  30.7 49.1 %all-to-all-start.1 = ((bf16[32,80,128]{2,1,0:T(8,128)(2,1)}), bf16[32,80,128]{2,1,0:T(8,128)(2,1)S(1)}, u32[]{:S(2)}, u32[]{:S(2)}) async-start(bf16[32,80,128]{2,1,0:T(8,128)(2,1)} %shard_map.66), calls=%async_computation.1 | async-start | bytes 1310720 | tf_op jit(solution)/shard_map/all_to_all | solution.py:33
  42.4 32.3 %collective-permute-start.2 = (bf16[256,2048]{1,0:T(8,128)(2,1)}, bf16[256,2048]{1,0:T(8,128)(2,1)S(1)}, u32[]{:S(2)}, u32[]{:S(2)}) collective-permute-start(bf16[256,2048]{1,0:T(8,128)(2,1)} %collective-permute-done.1.t2), channel_id=1, source_target_pairs={{0,1},{1,0},{2,3},{3,2},{4,5},{5,4},{6,7},{7,6},{8,9},{9,8},{10,11... | collective-permute-start | bytes 3145736 | tf_op jit(solution)/shard_map/ppermute | solution.py:29
  44.4 1.7 collective-permute-start.3
  46.2 16.1 %collective-permute-start.7 = (bf16[512,512]{1,0:T(8,128)(2,1)S(1)}, bf16[512,512]{1,0:T(8,128)(2,1)S(1)}, u32[]{:S(2)}, u32[]{:S(2)}) collective-permute-start(bf16[512,512]{1,0:T(8,128)(2,1)S(1)} %pad_maximum_fusion.w0), channel_id=1, source_target_pairs={{0,2},{2,4},{4,6},{6,0},{1,3},{3,5},{5,7},{7,1},{8,10},{10,12},{12... | collective-permute-start | bytes 1572872 | tf_op jit(solution)/shard_map/ppermute | solution.py:25
  47.3 25.6 %collective-permute-start.8 = (bf16[512,512]{1,0:T(8,128)(2,1)S(1)}, bf16[512,512]{1,0:T(8,128)(2,1)S(1)}, u32[]{:S(2)}, u32[]{:S(2)}) collective-permute-start(bf16[512,512]{1,0:T(8,128)(2,1)S(1)} %pad_maximum_fusion.w0), channel_id=1, source_target_pairs={{0,6},{2,0},{4,2},{6,4},{1,7},{3,1},{5,3},{7,5},{8,14},{10,8},{12,... | collective-permute-start | bytes 1572872 | tf_op jit(solution)/shard_map/ppermute | solution.py:25
  50.0 24.8 %collective-permute-start.9 = (bf16[512,512]{1,0:T(8,128)(2,1)S(1)}, bf16[512,512]{1,0:T(8,128)(2,1)S(1)}, u32[]{:S(2)}, u32[]{:S(2)}) collective-permute-start(bf16[512,512]{1,0:T(8,128)(2,1)S(1)} %pad_maximum_fusion.w0), channel_id=1, source_target_pairs={{0,4},{2,6},{4,0},{6,2},{1,5},{3,7},{5,1},{7,3},{8,12},{10,14},{12... | collective-permute-start | bytes 1572872 | tf_op jit(solution)/shard_map/ppermute | solution.py:25
  79.7 38.0 %all-to-all-start = ((bf16[16,128,256]{2,1,0:T(8,128)(2,1)}), bf16[16,128,256]{2,1,0:T(8,128)(2,1)S(1)}, u32[]{:S(2)}, u32[]{:S(2)}) async-start(bf16[16,128,256]{2,1,0:T(8,128)(2,1)} %shard_map.65), calls=%async_computation | async-start | bytes 2097152 | tf_op jit(solution)/shard_map/all_to_all | solution.py:33
  88.1 2.0 collective-permute-start.13
  140.2 57.9 %all-to-all-start.2 = ((bf16[32,128,128]{2,1,0:T(8,128)(2,1)}), bf16[32,128,128]{2,1,0:T(8,128)(2,1)S(1)}, u32[]{:S(2)}, u32[]{:S(2)}) async-start(bf16[32,128,128]{2,1,0:T(8,128)(2,1)} %shard_map.67), calls=%async_computation.2 | async-start | bytes 2097152 | tf_op jit(solution)/shard_map/all_to_all | solution.py:33
  145.5 2.0 collective-permute-start.14
  147.7 27.4 %collective-permute-start.15 = (bf16[256,2048]{1,0:T(8,128)(2,1)S(1)}, bf16[256,2048]{1,0:T(8,128)(2,1)S(1)}, u32[]{:S(2)}, u32[]{:S(2)}) collective-permute-start(bf16[256,2048]{1,0:T(8,128)(2,1)S(1)} %maximum_select_fusion.w0), channel_id=1, source_target_pairs={{0,2},{2,4},{4,6},{6,0},{1,3},{3,5},{5,7},{7,1},{8,10},{10,12},{12... | collective-permute-start | bytes 3145736 | tf_op jit(solution)/shard_map/ppermute | solution.py:25
  148.9 47.3 %collective-permute-start.16 = (bf16[256,2048]{1,0:T(8,128)(2,1)S(1)}, bf16[256,2048]{1,0:T(8,128)(2,1)S(1)}, u32[]{:S(2)}, u32[]{:S(2)}) collective-permute-start(bf16[256,2048]{1,0:T(8,128)(2,1)S(1)} %maximum_select_fusion.w0), channel_id=1, source_target_pairs={{0,6},{2,0},{4,2},{6,4},{1,7},{3,1},{5,3},{7,5},{8,14},{10,8},{12,... | collective-permute-start | bytes 3145736 | tf_op jit(solution)/shard_map/ppermute | solution.py:25
  151.3 45.9 %collective-permute-start.17 = (bf16[256,2048]{1,0:T(8,128)(2,1)S(1)}, bf16[256,2048]{1,0:T(8,128)(2,1)S(1)}, u32[]{:S(2)}, u32[]{:S(2)}) collective-permute-start(bf16[256,2048]{1,0:T(8,128)(2,1)S(1)} %maximum_select_fusion.w0), channel_id=1, source_target_pairs={{0,4},{2,6},{4,0},{6,2},{1,5},{3,7},{5,1},{7,3},{8,12},{10,14},{12... | collective-permute-start | bytes 3145736 | tf_op jit(solution)/shard_map/ppermute | solution.py:25
  202.5 2.7 %collective-permute-start.18 = (bf16[256,2048]{1,0:T(8,128)(2,1)S(1)}, bf16[256,2048]{1,0:T(8,128)(2,1)S(1)}, u32[]{:S(2)}, u32[]{:S(2)}) collective-permute-start(bf16[256,2048]{1,0:T(8,128)(2,1)S(1)} %shard_map.69), channel_id=1, source_target_pairs={{0,1},{1,0},{2,3},{3,2},{4,5},{5,4},{6,7},{7,6},{8,9},{9,8},{10,11... | collective-permute-start | bytes 3145736 | tf_op jit(solution)/shard_map/ppermute | solution.py:29
  (6 other events, 10.8 us)
